TPU v7x, 32 devices: a whole 2x2x4 slice. The times are simulated.
32 devices in a mesh: sp: 8 (over z, y), tp: 4 (over x, core).
Axes of the slice: x: 2, y: 2, z: 4, core: 2. Of those that a mesh axis runs over, the one named last changes fastest.
Arguments:
- frames: bfloat16 [4, 1024, 1024], P('tp', 'sp'), may hold values from -22 to 22
- norm_gain: float32 [1024], replicated, may hold values from 0.5 to 1.5
- conv_value_w: bfloat16 [1024, 512], P(None, 'tp'), may hold values from -0.1875 to 0.1875
- conv_gate_w: bfloat16 [1024, 512], P(None, 'tp'), may hold values from -0.1875 to 0.1875
- conv_taps: bfloat16 [31, 512], P(None, 'tp'), may hold values from -1 to 1
- conv_bias: float32 [512], P('tp'), may hold values from -1.2 to 1.2
- channel_gain: float32 [512], P('tp'), may hold values from 0.5 to 1.5
- channel_shift: float32 [512], P('tp'), may hold values from -1.2 to 1.2
- query_w: bfloat16 [1024, 1024], P(None, 'tp'), may hold values from -0.1875 to 0.1875
- forget_w: bfloat16 [1024, 1024], P(None, 'tp'), may hold values from -0.1875 to 0.1875
- input_w: bfloat16 [1024, 1024], P(None, 'tp'), may hold values from -0.1875 to 0.1875
- gate_w: bfloat16 [1024, 1024], P(None, 'tp'), may hold values from -0.1875 to 0.1875
- memory_rate: float32 [1024], P('tp'), may hold values from 0.5 to 32
- head_gain: float32 [1024], P('tp'), may hold values from 0.5 to 1.5
- conv_out_w: bfloat16 [512, 1024], P('tp'), may hold values from -0.1875 to 0.1875
- rec_out_w: bfloat16 [1024, 1024], P('tp'), may hold values from -0.125 to 0.125
Outputs:
- mixed: bfloat16 [4, 1024, 1024], P('tp', 'sp')
All inputs are finite; a program needn't handle non-finite values.
Results may differ from a plain program's by a relative error of at most 0.015.
The roundings to bfloat16 on the way count: a program that leaves them out, or rounds other values in their place, can miss the bound.
Values may be sent and summed in bfloat16 or wider, within the bound.
A program may use at most 64 MiB of HBM per device.

v0:
```python
import functools

import jax
import jax.numpy as jnp
from jax import lax
from jax.experimental import pallas as pl
from jax.experimental.pallas import tpu as pltpu
from jax.sharding import PartitionSpec as P

HEAD = 128
LANES = 128
EDGE = 32
EPS = 1e-06
MESH = pl.DeviceIdType.MESH
F32 = jnp.float32
BF16 = jnp.bfloat16


def flip(index, mask):
    out, bit = index, 1
    while bit <= mask:
        if mask & bit:
            out = out + bit - 2 * bit * ((index // bit) % 2)
        bit *= 2
    return out


def mm(a, b, dims):
    return lax.dot_general(a, b, (dims, ((), ())), preferred_element_type=F32)


def kernel(
    cfg,
    frames, norm_gain, cvw, cgw, taps, conv_bias, channel_gain, channel_shift,
    qw, fw, iw, gw, rate, head_gain, cow, row,
    out,
    gath, wbuf, ow, norm_v, taps_v, cb_v, cg_v, cs_v, rate_v, hg_v,
    gated, edges, ext, filt, stat, stat_in, conv_send, conv_in, rec_send, rec_in,
    grown_s, shrunk_s, value_s, gate_s, local_s, state, state_in, carry_out, carry_in, acc,
    loc_sem, fr_send, fr_recv, ow_send, ow_recv, ed_send, ed_recv, stt_send, stt_recv,
    ca_send, ca_recv, sm_send, sm_recv, cv_send, cv_recv, rc_send, rc_recv, wc_send, wc_recv,
):
    n_tp, n_sp, spt, d_conv, seq_total = cfg
    positions, depth = frames.shape[1], frames.shape[2]
    seqs = n_tp * spt
    conv_n, rec_n = cvw.shape[1], qw.shape[1]
    heads = rec_n // HEAD
    chunk = carry_out.shape[1]
    groups = carry_out.shape[0] // n_sp
    together = seqs // groups
    tp, sp = lax.axis_index("tp"), lax.axis_index("sp")

    barrier = pltpu.get_barrier_semaphore()
    for k in range(1, n_tp):
        pl.semaphore_signal(barrier, inc=1, device_id={"tp": flip(tp, k)}, device_id_type=MESH)
    for d in range(1, n_sp):
        pl.semaphore_signal(barrier, inc=1, device_id={"sp": (sp + d) % n_sp}, device_id_type=MESH)

    offsets = [0, conv_n, 2 * conv_n, 2 * conv_n + rec_n, 2 * conv_n + 2 * rec_n, 2 * conv_n + 3 * rec_n]
    copies = [pltpu.make_async_copy(frames, gath.at[0], loc_sem.at[0])]
    copies.append(pltpu.make_async_copy(norm_gain, norm_v, loc_sem.at[1]))
    for n, (ref, at) in enumerate(zip((cvw, cgw, qw, fw, iw, gw), offsets)):
        copies.append(
            pltpu.make_async_copy(ref, wbuf.at[:, pl.ds(at, ref.shape[1])], loc_sem.at[2 + n])
        )
    small = ((taps, taps_v), (conv_bias, cb_v), (channel_gain, cg_v), (channel_shift, cs_v), (rate, rate_v), (head_gain, hg_v))
    for n, (ref, to) in enumerate(small):
        copies.append(pltpu.make_async_copy(ref, to, loc_sem.at[8 + n]))
    copies.append(pltpu.make_async_copy(cow, ow.at[0, pl.ds(0, conv_n)], loc_sem.at[14]))
    copies.append(pltpu.make_async_copy(row, ow.at[0, pl.ds(conv_n, rec_n)], loc_sem.at[15]))
    for copy in copies:
        copy.start()

    def remote(src, dst, send, recv, **device):
        return pltpu.make_async_remote_copy(
            src_ref=src, dst_ref=dst, send_sem=send, recv_sem=recv, device_id=device, device_id_type=MESH
        )

    direct = [k for k in range(1, n_tp) if k % 2 == 0] + [1]
    fr = [None] * n_tp
    for k in range(1, n_tp):
        if k in direct:
            fr[k] = remote(frames, gath.at[k], fr_send.at[k], fr_recv.at[k], tp=flip(tp, k))
        else:
            fr[k] = remote(gath.at[k - 1], gath.at[k], fr_send.at[k], fr_recv.at[k], tp=flip(tp, 1))
    wt = [None] * n_tp
    for k in range(1, n_tp):
        source, to = (0, k) if k in direct else (k - 1, 1)
        wt[k] = remote(ow.at[source], ow.at[k], ow_send.at[k], ow_recv.at[k], tp=flip(tp, to))

    wc = {}
    for k in range(2, n_tp, 2):
        late, early = pl.ds(0, conv_n), pl.ds(conv_n, rec_n)
        wt[k] = remote(ow.at[0, early], ow.at[k, early], ow_send.at[k], ow_recv.at[k], tp=flip(tp, k))
        wc[k] = remote(ow.at[0, late], ow.at[k, late], wc_send.at[k], wc_recv.at[k], tp=flip(tp, k))

    pl.semaphore_wait(barrier, n_tp - 1 + n_sp - 1)
    for k in direct:
        fr[k].start()
    for copy in copies[14:]:
        copy.wait()
    for k in direct:
        wt[k].start()
    for copy in copies[:14]:
        copy.wait()

    t_row = lax.broadcasted_iota(jnp.int32, (positions, positions), 0)
    t_col = lax.broadcasted_iota(jnp.int32, (positions, positions), 1)
    causal = t_col <= t_row
    lower = jnp.where(causal, 1.0, 0.0).astype(BF16)
    lower3 = jnp.concatenate([lower, lower, lower], axis=1)
    rate_row = rate_v[...] / seq_total

    def state_copy(g, p):
        n = g * n_sp + p
        return remote(state.at[n], state_in.at[g * n_sp + sp], stt_send.at[n], stt_recv.at[g * n_sp + sp], sp=p)

    def state_from(g, j):
        n = g * n_sp + j
        return remote(state.at[n], state_in.at[n], stt_send.at[n], stt_recv.at[n], sp=j)

    def carry_copy(g, j):
        n = g * n_sp + j
        here = pl.multiple_of((g * n_sp + sp) * chunk, chunk)
        return remote(carry_out.at[n], carry_in.at[pl.ds(here, chunk)], ca_send.at[n], ca_recv.at[g * n_sp + sp], sp=j)

    def carry_from(g, j):
        n = g * n_sp + j
        return remote(carry_out.at[n], carry_in.at[pl.ds(n * chunk, chunk)], ca_send.at[n], ca_recv.at[n], sp=j)

    def scan(g):
        mine = g * n_sp + sp
        state_in[mine] = state[mine]
        carried = jnp.zeros((chunk, HEAD), F32)
        for j in range(n_sp):
            n = g * n_sp + j
            carry_out[n] = carried.astype(BF16)
            if j > 0:

                @pl.when(sp != j)
                def _():
                    carry_copy(g, j).start()

            if j < n_sp - 1:

                @pl.when(sp != j)
                def _():
                    state_from(g, j).wait_recv()

                carried = state_in[n, chunk : chunk + 1, :] * carried + state_in[n, 0:chunk, :]
        here = pl.multiple_of(mine * chunk, chunk)
        carry_in[pl.ds(here, chunk), :] = carry_out[mine]

    def edge_copy(q):
        return remote(
            gated.at[q, pl.ds(positions - EDGE, EDGE)], edges.at[q], ed_send.at[q], ed_recv.at[q], sp=(sp + 1) % n_sp
        )

    for k in range(n_tp):
        if k > 0:
            fr[k].wait_recv()
            if k % 2 == 0:
                fr[k + 1].start()
        for i in range(spt):
            q = k * spt + i
            x = gath[k, i].astype(F32)
            mean = jnp.mean(x * x, axis=-1, keepdims=True)
            normed = (x * lax.rsqrt(mean + EPS) * norm_v[...]).astype(BF16)

            def project(at, width):
                return mm(normed, wbuf[:, at : at + width], ((1,), (0,))).astype(BF16)

            conv_both = project(0, 2 * conv_n).astype(F32)
            gated_q = (conv_both[:, :conv_n] * jax.nn.sigmoid(conv_both[:, conv_n:])).astype(BF16)
            gated[q] = gated_q
            ext[q, EDGE : EDGE + positions] = gated_q.astype(F32)
            edge_copy(q).start()

            forget_raw = project(offsets[3], rec_n).astype(F32)
            in_gate = rate_row * jax.nn.sigmoid(-forget_raw)
            log_forget = jnp.log1p(-in_gate)
            hi = log_forget.astype(BF16)
            rest = log_forget - hi.astype(F32)
            mid = rest.astype(BF16)
            low = (rest - mid.astype(F32)).astype(BF16)
            cumulative = mm(lower3, jnp.concatenate([hi, mid, low], axis=0), ((1,), (0,)))
            last = cumulative[positions - 1 : positions, :]
            weighted = (in_gate * jnp.exp(last - cumulative)).astype(BF16)
            value = project(offsets[4], rec_n)
            value_s[q] = value
            last_decay = jnp.exp(last)
            for h in range(heads):
                pair = q * heads + h
                lanes = slice(h * HEAD, (h + 1) * HEAD)
                block = mm(value[:, lanes], weighted[:, lanes], ((0,), (0,)))
                rows_decay = jnp.broadcast_to(last_decay[:, lanes], (8, HEAD))
                for r in range(HEAD // chunk):
                    n = pair * (HEAD // chunk) + r
                    state[n, 0:chunk] = block[r * chunk : (r + 1) * chunk]
                    state[n, chunk : chunk + 8] = rows_decay
            if (q + 1) % together == 0:
                g = q // together
                for p in range(n_sp):

                    @pl.when(jnp.logical_and(sp != p, sp < n_sp - 1))
                    def _():
                        state_copy(g, p).start()

            shrunk_s[q] = (in_gate * jnp.exp(-cumulative)).astype(BF16)
            queries = project(offsets[2], rec_n).astype(F32)
            grown_s[q] = (queries * jnp.exp(cumulative)).astype(BF16)
            gate_s[q] = project(offsets[5], rec_n)
            if (q + 1) % together == 0 and q // together > 0:
                scan(q // together - 1)

    reach = taps.shape[0] - 1
    for q in range(seqs):
        edge_copy(q).wait_recv()
        ext[q, 0:EDGE] = jnp.where(sp > 0, edges[q].astype(F32), 0.0)
        total = jnp.broadcast_to(cb_v[...], (positions, conv_n))
        tap_rows = taps_v[...].astype(F32)
        for j in range(reach + 1):
            start = EDGE - reach + j
            total = total + tap_rows[j : j + 1, :] * ext[q, start : start + positions, :]
        filt[q] = total
        lane = lax.broadcasted_iota(jnp.int32, (positions, LANES), 1)
        sums = jnp.sum(total, axis=-1, keepdims=True)
        squares = jnp.sum(total * total, axis=-1, keepdims=True)
        table = jnp.where(lane == 0, sums, jnp.where(lane == 1, squares, 0.0))
        stat[q] = jnp.transpose(table)[0:8, :]

    def stat_copy(k):
        return remote(stat, stat_in.at[k], sm_send.at[k], sm_recv.at[k], tp=flip(tp, k))

    for k in range(1, n_tp):
        stat_copy(k).start()
    for k in wc:
        wc[k].start()

    scan(groups - 1)

    for q in range(seqs):
        for h in range(heads):
            lanes = slice(h * HEAD, (h + 1) * HEAD)
            scores = mm(grown_s[q, :, lanes], shrunk_s[q, :, lanes], ((1,), (1,)))
            scores = jnp.where(causal, scores, 0.0).astype(BF16)
            local_s[q, :, lanes] = mm(scores, value_s[q, :, lanes], ((1,), (0,)))

    for k in range(1, n_tp):
        stat_copy(k).wait_recv()

    def conv_copy(k):
        return remote(conv_send.at[k], conv_in.at[k], cv_send.at[k], cv_recv.at[k], tp=flip(tp, k))

    def rec_copy(k):
        return remote(rec_send.at[k], rec_in.at[k], rc_send.at[k], rc_recv.at[k], tp=flip(tp, k))

    order = list(range(n_tp - 1, -1, -1))
    for k in order:
        for i in range(spt):
            q = k * spt + i
            both = stat[q]
            for d in range(1, n_tp):
                both = both + stat_in[d, (k ^ d) * spt + i]
            both = both / d_conv
            table = jnp.concatenate([both, jnp.zeros((LANES - 8, positions), F32)], axis=0)
            table = jnp.transpose(table)
            row_mean = table[:, 0:1]
            row_var = table[:, 1:2] - row_mean * row_mean
            scaled = (filt[q] - row_mean) * lax.rsqrt(row_var + EPS) * cg_v[...] + cs_v[...]
            result = (scaled * jax.nn.sigmoid(scaled)).astype(BF16)
            rows = slice(i * positions, (i + 1) * positions)
            if k == 0:
                conv_in[0, rows] = result
            else:
                conv_send[k, rows] = result
        if k > 0:
            conv_copy(k).start()

    @pl.when(sp == 0)
    def _():
        carry_in[...] = jnp.zeros_like(carry_in)

    arrived = set()
    for k in [1, 0] + list(range(2, n_tp)):
        for i in range(spt):
            q = k * spt + i
            rows = slice(i * positions, (i + 1) * positions)
            g = q // together
            for j in range(n_sp if g not in arrived else 0):

                @pl.when(jnp.logical_and(sp != j, sp > 0))
                def _():
                    carry_from(g, j).wait_recv()

            arrived.add(g)
            for h in range(heads):
                pair = q * heads + h
                lanes = slice(h * HEAD, (h + 1) * HEAD)
                rec_raw = local_s[q, :, lanes] + mm(
                    grown_s[q, :, lanes], carry_in[pair * HEAD : (pair + 1) * HEAD, :], ((1,), (1,))
                )
                mean = jnp.mean(rec_raw * rec_raw, axis=-1, keepdims=True)
                rec_norm = rec_raw * lax.rsqrt(mean + EPS) * hg_v[:, lanes]
                gate = gate_s[q, :, lanes].astype(F32)
                result = (rec_norm * (gate * jax.nn.sigmoid(gate))).astype(BF16)
                if k == 0:
                    rec_in[0, rows, lanes] = result
                else:
                    rec_send[k, rows, lanes] = result
        if k > 0:
            rec_copy(k).start()

    for k in range(2, n_tp, 2):
        wt[k].wait_recv()
        wc[k].wait_recv()
        wt[k + 1].start()
    if n_tp > 1:
        wt[1].wait_recv()
    for n, k in enumerate(range(n_tp)):
        if k > 0:
            if k % 2 == 1 and k > 1:
                wt[k].wait_recv()
            conv_copy(k).wait_recv()
            rec_copy(k).wait_recv()
        part = mm(conv_in[k], ow[k, 0:conv_n, :], ((1,), (0,))) + mm(
            rec_in[k], ow[k, conv_n : conv_n + rec_n, :], ((1,), (0,))
        )
        if k == 0:
            acc[...] = part
        elif k < n_tp - 1:
            acc[...] += part
        else:
            out[...] = (acc[...] + part).astype(BF16).reshape(out.shape)

    for k in range(1, n_tp):
        fr[k].wait_send()
        wt[k].wait_send()
        if k in wc:
            wc[k].wait_send()
        stat_copy(k).wait_send()
        conv_copy(k).wait_send()
        rec_copy(k).wait_send()
    for q in range(seqs):
        edge_copy(q).wait_send()
    for g in range(groups):
        for p in range(n_sp):

            @pl.when(jnp.logical_and(sp != p, sp < n_sp - 1))
            def _():
                state_copy(g, p).wait_send()

            if p > 0:

                @pl.when(sp != p)
                def _():
                    carry_copy(g, p).wait_send()


def wide(array, axis):
    extra = -array.shape[axis] % LANES
    if extra == 0:
        return array
    pads = [(0, 0)] * array.ndim
    pads[axis] = (0, extra)
    return jnp.pad(array, pads)


def local(
    n_tp, n_sp, frames, norm_gain, conv_value_w, conv_gate_w, conv_taps, conv_bias, channel_gain, channel_shift,
    query_w, forget_w, input_w, gate_w, memory_rate, head_gain, conv_out_w, rec_out_w,
):
    d_conv = conv_value_w.shape[1] * n_tp
    spt, positions, depth = frames.shape
    conv_value_w, conv_gate_w, conv_taps = (wide(a, 1) for a in (conv_value_w, conv_gate_w, conv_taps))
    conv_bias, channel_gain, channel_shift, conv_out_w = (
        wide(a, 0) for a in (conv_bias, channel_gain, channel_shift, conv_out_w)
    )
    conv_n, rec_n = conv_value_w.shape[1], query_w.shape[1]
    out_n = rec_out_w.shape[1]
    seqs = n_tp * spt
    heads = rec_n // HEAD
    pairs = seqs * heads
    together = 1
    while together < seqs and together * heads * HEAD // n_sp < 16:
        together *= 2
    groups = seqs // together
    chunk = together * heads * HEAD // n_sp
    slots = groups * n_sp
    width = conv_n * 2 + rec_n * 4
    rows = spt * positions
    vm = pltpu.VMEM
    sem = pltpu.SemaphoreType.DMA
    scratch = [
        vm((n_tp, spt, positions, depth), BF16),
        vm((depth, width), BF16),
        vm((n_tp, conv_n + rec_n, out_n), BF16),
        vm((1, depth), F32),
        vm(conv_taps.shape, BF16),
        vm((1, conv_n), F32),
        vm((1, conv_n), F32),
        vm((1, conv_n), F32),
        vm((1, rec_n), F32),
        vm((1, rec_n), F32),
        vm((seqs, positions, conv_n), BF16),
        vm((seqs, EDGE, conv_n), BF16),
        vm((seqs, EDGE + positions, conv_n), F32),
        vm((seqs, positions, conv_n), F32),
        vm((seqs, 8, positions), F32),
        vm((n_tp, seqs, 8, positions), F32),
        vm((n_tp, rows, conv_n), BF16),
        vm((n_tp, rows, conv_n), BF16),
        vm((n_tp, rows, rec_n), BF16),
        vm((n_tp, rows, rec_n), BF16),
        vm((seqs, positions, rec_n), BF16),
        vm((seqs, positions, rec_n), BF16),
        vm((seqs, positions, rec_n), BF16),
        vm((seqs, positions, rec_n), BF16),
        vm((seqs, positions, rec_n), F32),
        vm((slots, chunk + 8, HEAD), F32),
        vm((slots, chunk + 8, HEAD), F32),
        vm((slots, chunk, HEAD), BF16),
        vm((pairs * HEAD, HEAD), BF16),
        vm((rows, out_n), F32),
        sem((16,)),
        sem((n_tp,)), sem((n_tp,)),
        sem((n_tp,)), sem((n_tp,)),
        sem((seqs,)), sem((seqs,)),
        sem((slots,)), sem((slots,)),
        sem((slots,)), sem((slots,)),
        sem((n_tp,)), sem((n_tp,)),
        sem((n_tp,)), sem((n_tp,)),
        sem((n_tp,)), sem((n_tp,)),
        sem((n_tp,)), sem((n_tp,)),
    ]
    return pl.pallas_call(
        functools.partial(kernel, (n_tp, n_sp, spt, d_conv, positions * n_sp)),
        out_shape=jax.ShapeDtypeStruct((spt, positions, out_n), BF16),
        in_specs=[pl.BlockSpec(memory_space=pltpu.HBM)] * 16,
        out_specs=pl.BlockSpec(memory_space=pltpu.VMEM),
        scratch_shapes=scratch,
        compiler_params=pltpu.CompilerParams(
            collective_id=0, has_side_effects=True, vmem_limit_bytes=56 * 1024 * 1024
        ),
    )(
        frames, norm_gain[None], conv_value_w, conv_gate_w, conv_taps, conv_bias[None], channel_gain[None],
        channel_shift[None], query_w, forget_w, input_w, gate_w, memory_rate[None], head_gain[None],
        conv_out_w, rec_out_w,
    )


def solution(mesh):
    placed = (
        P("tp", "sp", None),
        P(),
        P(None, "tp"),
        P(None, "tp"),
        P(None, "tp"),
        P("tp"),
        P("tp"),
        P("tp"),
        P(None, "tp"),
        P(None, "tp"),
        P(None, "tp"),
        P(None, "tp"),
        P("tp"),
        P("tp"),
        P("tp", None),
        P("tp", None),
    )
    return jax.shard_map(
        functools.partial(local, mesh.shape["tp"], mesh.shape["sp"]),
        mesh=mesh, in_specs=placed, out_specs=P("tp", "sp", None), check_vma=False,
    )
```

profile of v0, /device:TPU:0, one launch (start us, length us, event | category | flops | bytes accessed | tf_op | source)
XLA Modules:
  0.0 39.8 jit_solution(11979080011656976947)
XLA Ops:
  0.0 38.2 %shard_map.154 = bf16[1,128,1024]{2,1,0:T(8,128)(2,1)} custom-call(bf16[1,128,1024]{2,1,0:T(8,128)(2,1)} %frames.1, f32[1,1024]{1,0:T(1,128)} %bitcast.6, bf16[1024,128]{1,0:T(8,128)(2,1)} %cvw.1, bf16[1024,128]{1,0:T(8,128)(2,1)} %cgw.1, bf16[31,128]{1,0:T(8,128)(2,1)} %taps.1, f32[1,128]{1,0:T(1,128)} %bitcast.9, f32[1,128]{1,0:T(1,128)} %bitcast.10, ...), custom_call_target="tpu_custom_call" | custom-call | tf_op jit(solution)/shard_map/pallas_call | solution.py:436
  38.2 1.7 %copy.18 = bf16[1,128,1024]{2,1,0:T(8,128)(2,1)} copy(bf16[1,128,1024]{2,1,0:T(8,128)(2,1)} %shard_map.154) | data formatting | bytes 524288
where the time goes:
time: 40 us; the launch traced here: 39.8 us
  Pallas kernels  38.2 us (96%)
  local copies, waits for them, and re-layouts  1.67 us (4%)
    pallas_call x1, Pallas kernels, local(): pl.pallas_call(functools.partial(kernel, (n_tp, n_sp, spt, d_conv, positi...  38.2 us
    unnamed x1, local copies, waits for them, and re-layouts  1.67 us

commit v1 on v0

v1 whole, which is shorter than its diff:
```python
import functools

import jax
import jax.numpy as jnp
from jax import lax
from jax.experimental import pallas as pl
from jax.experimental.pallas import tpu as pltpu
from jax.sharding import PartitionSpec as P

HEAD = 128
LANES = 128
EDGE = 32
PACK = 16
COLS = 256
EPS = 1e-06
MESH = pl.DeviceIdType.MESH
F32 = jnp.float32
BF16 = jnp.bfloat16


def flip(index, mask):
    out, bit = index, 1
    while bit <= mask:
        if mask & bit:
            out = out + bit - 2 * bit * ((index // bit) % 2)
        bit *= 2
    return out


def mm(a, b, dims=((1,), (0,))):
    return lax.dot_general(a, b, (dims, ((), ())), preferred_element_type=F32)


def split3(value):
    hi = value.astype(BF16)
    rest = value - hi.astype(F32)
    mid = rest.astype(BF16)
    return hi, mid, (rest - mid.astype(F32)).astype(BF16)


def kernel(
    cfg,
    frames, norm_gain, cvw, cgw, taps, conv_bias, channel_gain, channel_shift,
    qw, fw, iw, gw, rate, head_gain, cow, row,
    out,
    gath, norm_v, wf, wi, wc, wq, wg, taps_v, cb_v, cg_v, cs_v, rate_v, hg_v, ow,
    nrm, ecum_s, gated, edges, ext, filt, stat, stat_in, cvo, rco,
    grown_s, shrunk_s, value_s, gate_s, local_s, st, st_in, carry_out, carry_in, acc, psend, precv,
    up, loc_sem, d2_send, d2_recv, fr_send, fr_recv, ed_send, ed_recv, stt_send, stt_recv,
    ca_send, ca_recv, sm_send, sm_recv, pt_send, pt_recv,
):
    n_tp, n_sp, d_conv, seq_total, owners = cfg
    positions = frames.shape[1]
    conv_n, rec_n = cvw.shape[1], qw.shape[1]
    heads = rec_n // HEAD
    nx = n_tp // 2
    chunk = carry_out.shape[2]
    stride = n_sp // owners
    pieces = acc.shape[1]
    tp, sp = lax.axis_index("tp"), lax.axis_index("sp")
    core = tp % 2
    owner = sp // stride

    barrier = pltpu.get_barrier_semaphore()
    pl.semaphore_signal(barrier, inc=1, device_id={"tp": flip(tp, 1)}, device_id_type=MESH)
    for k in range(1, nx):
        pl.semaphore_signal(barrier, inc=1, device_id={"tp": flip(tp, 2 * k)}, device_id_type=MESH)
    for d in range(1, n_sp):

        @pl.when(sp + d < n_sp)
        def _():
            pl.semaphore_signal(barrier, inc=1, device_id={"sp": sp + d}, device_id_type=MESH)

    mine = pltpu.make_async_copy(frames, gath.at[pl.ds(0, 1)], loc_sem.at[0])
    gain_in = pltpu.make_async_copy(norm_gain, norm_v, loc_sem.at[1])

    def remote(src, dst, send, recv, **device):
        return pltpu.make_async_remote_copy(
            src_ref=src, dst_ref=dst, send_sem=send, recv_sem=recv, device_id=device, device_id_type=MESH
        )

    rec_at = 2 * conv_n
    table = (
        ("f", fw, wf.at[0], wf.at[1]),
        ("rate", rate, rate_v.at[0], rate_v.at[1]),
        ("i", iw, wi.at[0], wi.at[1]),
        ("cv", cvw, wc.at[0, :, pl.ds(0, conv_n)], wc.at[1, :, pl.ds(0, conv_n)]),
        ("cg", cgw, wc.at[0, :, pl.ds(conv_n, conv_n)], wc.at[1, :, pl.ds(conv_n, conv_n)]),
        ("q", qw, wq.at[0], wq.at[1]),
        ("g", gw, wg.at[0], wg.at[1]),
        ("taps", taps, taps_v.at[0], taps_v.at[1]),
        ("cb", conv_bias, cb_v.at[0], cb_v.at[1]),
        ("gain", channel_gain, cg_v.at[0], cg_v.at[1]),
        ("shift", channel_shift, cs_v.at[0], cs_v.at[1]),
        ("hg", head_gain, hg_v.at[0], hg_v.at[1]),
        ("co", cow, ow.at[pl.ds(0, conv_n)], ow.at[pl.ds(conv_n, conv_n)]),
        ("ro", row, ow.at[pl.ds(rec_at, rec_n)], ow.at[pl.ds(rec_at + rec_n, rec_n)]),
    )
    names = [entry[0] for entry in table]
    load = {}
    swap = {}
    for n, (name, ref, here, there) in enumerate(table):
        load[name] = pltpu.make_async_copy(ref, here, loc_sem.at[2 + n])
        swap[name] = remote(here, there, d2_send.at[n], d2_recv.at[n], tp=flip(tp, 1))
    mine.start()
    gain_in.start()
    for name in names:
        load[name].start()

    fr = [None] * nx
    for k in range(1, nx):
        fr[k] = remote(gath.at[0], gath.at[k], fr_send.at[k], fr_recv.at[k], tp=flip(tp, 2 * k))

    mine.wait()
    pl.semaphore_wait(barrier, nx + sp)

    @pl.when(core == 0)
    def _():
        for k in range(1, nx):
            fr[k].start()

    for d in range(1, n_sp):

        @pl.when(sp >= d)
        def _():
            pl.semaphore_signal(up, inc=1, device_id={"sp": sp - d}, device_id_type=MESH)

    for name in names:
        load[name].wait()
        swap[name].start()
    gain_in.wait()

    t_row = lax.broadcasted_iota(jnp.int32, (positions, positions), 0)
    t_col = lax.broadcasted_iota(jnp.int32, (positions, positions), 1)
    causal = t_col <= t_row
    lower = jnp.where(causal, 1.0, 0.0).astype(BF16)
    lower3 = jnp.concatenate([lower, lower, lower], axis=1)
    tile_row = lax.broadcasted_iota(jnp.int32, (PACK, HEAD), 0)

    def norm(k):
        x = gath[k].astype(F32)
        mean = jnp.mean(x * x, axis=-1, keepdims=True)
        nrm[k] = (x * lax.rsqrt(mean + EPS) * norm_v[...]).astype(BF16)

    def project(k, weight):
        return mm(nrm[k], weight[...]).astype(BF16)

    def lanes_of(half):
        return slice(half * rec_n, (half + 1) * rec_n)

    def states(k, half):
        cols = lanes_of(half)
        forget_raw = project(k, wf.at[half]).astype(F32)
        in_gate = (rate_v[half] / seq_total) * jax.nn.sigmoid(-forget_raw)
        hi, mid, low = split3(jnp.log1p(-in_gate))
        cumulative = mm(lower3, jnp.concatenate([hi, mid, low], axis=0))
        last = cumulative[positions - 1 : positions, :]
        weighted = (in_gate * jnp.exp(last - cumulative)).astype(BF16)
        value = project(k, wi.at[half])
        value_s[k, :, cols] = value
        last_decay = jnp.exp(last)
        for h in range(heads):
            lanes = slice(h * HEAD, (h + 1) * HEAD)
            block = mm(value[:, lanes], weighted[:, lanes], ((0,), (0,))).astype(BF16)
            hi, mid, low = split3(last_decay[:, lanes])
            rows = jnp.where(
                tile_row == 0, hi.astype(F32), jnp.where(tile_row == 1, mid.astype(F32), low.astype(F32))
            ).astype(BF16)
            for r in range(HEAD // chunk):
                n = (half * heads + h) * (HEAD // chunk) + r
                st[k, n, 0:chunk] = block[r * chunk : (r + 1) * chunk]
                st[k, n, chunk : chunk + PACK] = rows
        shrunk_s[k, :, cols] = (in_gate * jnp.exp(-cumulative)).astype(BF16)
        ecum_s[k, :, cols] = jnp.exp(cumulative)

    def gates(k, half):
        both = project(k, wc.at[half]).astype(F32)
        result = (both[:, :conv_n] * jax.nn.sigmoid(both[:, conv_n:])).astype(BF16)
        cols = slice(half * conv_n, (half + 1) * conv_n)
        gated[k, :, cols] = result
        ext[k, EDGE : EDGE + positions, cols] = result.astype(F32)

    def outer(k, half):
        cols = lanes_of(half)
        queries = project(k, wq.at[half]).astype(F32)
        grown_s[k, :, cols] = (queries * ecum_s[k, :, cols]).astype(BF16)
        gate_s[k, :, cols] = project(k, wg.at[half])

    def within(k):
        for h in range(2 * heads):
            lanes = slice(h * HEAD, (h + 1) * HEAD)
            scores = mm(grown_s[k, :, lanes], shrunk_s[k, :, lanes], ((1,), (1,)))
            scores = jnp.where(causal, scores, 0.0).astype(BF16)
            local_s[k, :, lanes] = mm(scores, value_s[k, :, lanes])

    def state_copy(k, o):
        return remote(
            st.at[k, o], st_in.at[k, sp], stt_send.at[k * owners + o], stt_recv.at[k * n_sp + sp], sp=o * stride
        )

    def state_from(k, j):
        return remote(st.at[k, 0], st_in.at[k, j], stt_send.at[k * owners], stt_recv.at[k * n_sp + j], sp=j)

    def send_states(k):
        for o in range(owners):

            @pl.when(jnp.logical_and(sp != o * stride, sp < n_sp - 1))
            def _():
                state_copy(k, o).start()

    def carry_copy(k, j):
        here = pl.ds(pl.multiple_of(owner * chunk, chunk), chunk)
        return remote(
            carry_out.at[k, j], carry_in.at[k, here], ca_send.at[k * n_sp + j], ca_recv.at[k * owners + owner], sp=j
        )

    def carry_from(k, o):
        return remote(
            carry_out.at[k, 0], carry_in.at[k, pl.ds(o * chunk, chunk)],
            ca_send.at[k * n_sp], ca_recv.at[k * owners + o], sp=o * stride,
        )

    def owned(body):
        if stride == 1:
            body()
        else:
            pl.when(sp % stride == 0)(body)

    def scan(k):
        def body():
            st_in[k, sp] = st[k, owner]
            carried = jnp.zeros((chunk, HEAD), F32)
            for j in range(n_sp):
                carry_out[k, j] = carried.astype(BF16)
                if j > 0:

                    @pl.when(sp != j)
                    def _():
                        carry_copy(k, j).start()

                if j < n_sp - 1:

                    @pl.when(sp != j)
                    def _():
                        state_from(k, j).wait_recv()

                    decay = st_in[k, j, chunk : chunk + PACK].astype(F32)
                    decay = decay[0:1] + decay[1:2] + decay[2:3]
                    carried = decay * carried + st_in[k, j, 0:chunk].astype(F32)
            here = pl.multiple_of(owner * chunk, chunk)
            carry_in[k, pl.ds(here, chunk), :] = carry_out[k, sp]

        owned(body)

    def wait_carry(k):
        for o in range(owners):

            @pl.when(jnp.logical_and(sp != o * stride, sp > 0))
            def _():
                carry_from(k, o).wait_recv()

    def edge_copy(k):
        return remote(gated.at[k, pl.ds(positions - EDGE, EDGE)], edges.at[k], ed_send.at[k], ed_recv.at[k], sp=sp + 1)

    def send_edge(k):
        @pl.when(sp < n_sp - 1)
        def _():
            edge_copy(k).start()

    def stat_copy(k, j):
        return remote(
            stat.at[k], stat_in.at[j, k ^ j], sm_send.at[j * nx + k], sm_recv.at[j * nx + (k ^ j)], tp=flip(tp, 2 * j)
        )

    def stat_from(k, j):
        return remote(stat.at[k], stat_in.at[j, k], sm_send.at[j * nx + k], sm_recv.at[j * nx + k], tp=flip(tp, 2 * j))

    reach = taps.shape[0] - 1

    def conv(k):
        @pl.when(sp > 0)
        def _():
            edge_copy(k).wait_recv()
            ext[k, 0:EDGE] = edges[k].astype(F32)

        @pl.when(sp == 0)
        def _():
            ext[k, 0:EDGE] = jnp.zeros((EDGE, 2 * conv_n), F32)

        sums = squares = 0.0
        for half in range(2):
            cols = slice(half * conv_n, (half + 1) * conv_n)
            total = jnp.broadcast_to(cb_v[half], (positions, conv_n))
            tap_rows = taps_v[half].astype(F32)
            for j in range(reach + 1):
                start = EDGE - reach + j
                total = total + tap_rows[j : j + 1, :] * ext[k, start : start + positions, cols]
            filt[k, :, cols] = total
            sums = sums + jnp.sum(total, axis=-1, keepdims=True)
            squares = squares + jnp.sum(total * total, axis=-1, keepdims=True)
        lane = lax.broadcasted_iota(jnp.int32, (positions, LANES), 1)
        both = jnp.where(lane == 0, sums, jnp.where(lane == 1, squares, 0.0))
        stat[k] = jnp.transpose(both)[0:8, :]
        for j in range(1, nx):
            stat_copy(k, j).start()

    def conv_norm(k):
        both = stat[k]
        for j in range(1, nx):
            stat_from(k, j).wait_recv()
            both = both + stat_in[j, k]
        both = both / d_conv
        turned = jnp.transpose(jnp.concatenate([both, jnp.zeros((LANES - 8, positions), F32)], axis=0))
        row_mean = turned[:, 0:1]
        row_var = turned[:, 1:2] - row_mean * row_mean
        scale = lax.rsqrt(row_var + EPS)
        for half in range(2):
            cols = slice(half * conv_n, (half + 1) * conv_n)
            scaled = (filt[k, :, cols] - row_mean) * scale * cg_v[half] + cs_v[half]
            cvo[k, :, cols] = (scaled * jax.nn.sigmoid(scaled)).astype(BF16)
        for n in range(pieces):
            acc[k, n] = mm(cvo[k], ow[0:rec_at, n * COLS : (n + 1) * COLS])

    def finish(k):
        wait_carry(k)
        for h in range(2 * heads):
            lanes = slice(h * HEAD, (h + 1) * HEAD)
            rec_raw = local_s[k, :, lanes] + mm(
                grown_s[k, :, lanes], carry_in[k, h * HEAD : (h + 1) * HEAD, :], ((1,), (1,))
            )
            mean = jnp.mean(rec_raw * rec_raw, axis=-1, keepdims=True)
            gain = hg_v[h // heads][:, (h % heads) * HEAD : (h % heads + 1) * HEAD]
            rec_norm = rec_raw * lax.rsqrt(mean + EPS) * gain
            gate = gate_s[k, :, lanes].astype(F32)
            rco[k, :, lanes] = (rec_norm * (gate * jax.nn.sigmoid(gate))).astype(BF16)

    def part_copy(k, n):
        return remote(
            psend.at[k, n], precv.at[k, n], pt_send.at[k * pieces + n], pt_recv.at[k * pieces + n], tp=flip(tp, 2 * k)
        )

    def produce(k):
        for n in range(pieces):
            part = acc[k, n] + mm(rco[k], ow[rec_at : rec_at + 2 * rec_n, n * COLS : (n + 1) * COLS])
            if k == 0:
                acc[k, n] = part
            else:
                psend[k, n] = part.astype(BF16)
                part_copy(k, n).start()

    @pl.when(sp == 0)
    def _():
        carry_in[...] = jnp.zeros_like(carry_in)

    norm(0)
    states(0, 0)
    gates(0, 0)
    outer(0, 0)

    @pl.when(core == 1)
    def _():
        for k in range(1, nx):
            fr[k].start()

    for name in ("f", "rate", "i"):
        swap[name].wait_recv()
    states(0, 1)

    @pl.when(sp < n_sp - 1)
    def _():
        pl.semaphore_wait(up, n_sp - 1 - sp)

    send_states(0)
    for name in ("cv", "cg"):
        swap[name].wait_recv()
    gates(0, 1)
    send_edge(0)
    for name in ("q", "g"):
        swap[name].wait_recv()
    outer(0, 1)
    within(0)
    for name in ("taps", "cb", "gain", "shift", "hg", "co", "ro"):
        swap[name].wait_recv()

    for k in range(1, nx):
        fr[k].wait_recv()
        norm(k)
        states(k, 0)
        states(k, 1)
        send_states(k)
        gates(k, 0)
        gates(k, 1)
        send_edge(k)
        outer(k, 0)
        outer(k, 1)
        scan(k - 1)
        conv(k - 1)
        within(k)
    scan(nx - 1)
    conv(nx - 1)
    finish(0)
    for k in range(nx):
        conv_norm(k)
    for k in range(1, nx):
        finish(k)
        produce(k)
    produce(0)
    for n in range(pieces):
        total = acc[0, n]
        for k in range(1, nx):
            part_copy(k, n).wait_recv()
            total = total + precv[k, n].astype(F32)
        out[0, :, n * COLS : (n + 1) * COLS] = total.astype(BF16)

    for name in names:
        swap[name].wait_send()
    for k in range(1, nx):
        fr[k].wait_send()
        for n in range(pieces):
            part_copy(k, n).wait_send()
    for k in range(nx):
        for j in range(1, nx):
            stat_copy(k, j).wait_send()

        @pl.when(sp < n_sp - 1)
        def _():
            edge_copy(k).wait_send()

        for o in range(owners):

            @pl.when(jnp.logical_and(sp != o * stride, sp < n_sp - 1))
            def _():
                state_copy(k, o).wait_send()

        def drain():
            for j in range(1, n_sp):

                @pl.when(sp != j)
                def _():
                    carry_copy(k, j).wait_send()

        owned(drain)


def wide(array, axis):
    extra = -array.shape[axis] % LANES
    if extra == 0:
        return array
    pads = [(0, 0)] * array.ndim
    pads[axis] = (0, extra)
    return jnp.pad(array, pads)


def local(
    n_tp, n_sp, frames, norm_gain, conv_value_w, conv_gate_w, conv_taps, conv_bias, channel_gain, channel_shift,
    query_w, forget_w, input_w, gate_w, memory_rate, head_gain, conv_out_w, rec_out_w,
):
    d_conv = conv_value_w.shape[1] * n_tp
    spt, positions, depth = frames.shape
    conv_value_w, conv_gate_w, conv_taps = (wide(a, 1) for a in (conv_value_w, conv_gate_w, conv_taps))
    conv_bias, channel_gain, channel_shift, conv_out_w = (
        wide(a, 0) for a in (conv_bias, channel_gain, channel_shift, conv_out_w)
    )
    conv_n, rec_n = conv_value_w.shape[1], query_w.shape[1]
    out_n = rec_out_w.shape[1]
    assert spt == 1 and n_tp % 2 == 0 and positions == LANES and out_n % COLS == 0
    nx = n_tp // 2
    state_rows = 2 * rec_n
    owners = min(n_sp, state_rows // PACK)
    chunk = state_rows // owners
    pieces = out_n // COLS
    vm = pltpu.VMEM
    sem = pltpu.SemaphoreType.DMA
    scratch = [
        vm((nx, positions, depth), BF16),
        vm((1, depth), F32),
        vm((2, depth, rec_n), BF16),
        vm((2, depth, rec_n), BF16),
        vm((2, depth, 2 * conv_n), BF16),
        vm((2, depth, rec_n), BF16),
        vm((2, depth, rec_n), BF16),
        vm((2,) + conv_taps.shape, BF16),
        vm((2, 1, conv_n), F32),
        vm((2, 1, conv_n), F32),
        vm((2, 1, conv_n), F32),
        vm((2, 1, rec_n), F32),
        vm((2, 1, rec_n), F32),
        vm((2 * conv_n + 2 * rec_n, out_n), BF16),
        vm((nx, positions, depth), BF16),
        vm((nx, positions, 2 * rec_n), F32),
        vm((nx, positions, 2 * conv_n), BF16),
        vm((nx, EDGE, 2 * conv_n), BF16),
        vm((nx, EDGE + positions, 2 * conv_n), F32),
        vm((nx, positions, 2 * conv_n), F32),
        vm((nx, 8, positions), F32),
        vm((nx, nx, 8, positions), F32),
        vm((nx, positions, 2 * conv_n), BF16),
        vm((nx, positions, 2 * rec_n), BF16),
        vm((nx, positions, 2 * rec_n), BF16),
        vm((nx, positions, 2 * rec_n), BF16),
        vm((nx, positions, 2 * rec_n), BF16),
        vm((nx, positions, 2 * rec_n), BF16),
        vm((nx, positions, 2 * rec_n), F32),
        vm((nx, owners, chunk + PACK, HEAD), BF16),
        vm((nx, n_sp, chunk + PACK, HEAD), BF16),
        vm((nx, n_sp, chunk, HEAD), BF16),
        vm((nx, state_rows, HEAD), BF16),
        vm((nx, pieces, positions, COLS), F32),
        vm((nx, pieces, positions, COLS), BF16),
        vm((nx, pieces, positions, COLS), BF16),
        pltpu.SemaphoreType.REGULAR,
        sem((16,)),
        sem((14,)), sem((14,)),
        sem((nx,)), sem((nx,)),
        sem((nx,)), sem((nx,)),
        sem((nx * owners,)), sem((nx * n_sp,)),
        sem((nx * n_sp,)), sem((nx * owners,)),
        sem((nx * nx,)), sem((nx * nx,)),
        sem((nx * pieces,)), sem((nx * pieces,)),
    ]
    return pl.pallas_call(
        functools.partial(kernel, (n_tp, n_sp, d_conv, positions * n_sp, owners)),
        out_shape=jax.ShapeDtypeStruct((spt, positions, out_n), BF16),
        in_specs=[pl.BlockSpec(memory_space=pltpu.HBM)] * 16,
        out_specs=pl.BlockSpec(memory_space=pltpu.VMEM),
        scratch_shapes=scratch,
        compiler_params=pltpu.CompilerParams(
            collective_id=0, has_side_effects=True, vmem_limit_bytes=56 * 1024 * 1024
        ),
    )(
        frames, norm_gain[None], conv_value_w, conv_gate_w, conv_taps, conv_bias[None], channel_gain[None],
        channel_shift[None], query_w, forget_w, input_w, gate_w, memory_rate[None], head_gain[None],
        conv_out_w, rec_out_w,
    )


def solution(mesh):
    placed = (
        P("tp", "sp", None),
        P(),
        P(None, "tp"),
        P(None, "tp"),
        P(None, "tp"),
        P("tp"),
        P("tp"),
        P("tp"),
        P(None, "tp"),
        P(None, "tp"),
        P(None, "tp"),
        P(None, "tp"),
        P("tp"),
        P("tp"),
        P("tp", None),
        P("tp", None),
    )
    return jax.shard_map(
        functools.partial(local, mesh.shape["tp"], mesh.shape["sp"]),
        mesh=mesh, in_specs=placed, out_specs=P("tp", "sp", None), check_vma=False,
    )
```

time: 40 us -> 34.2 us (0.86)
  the two profiles are of different devices: /device:TPU:0 before, /device:TPU:24 now
where the time goes in v1:
time: 34.2 us; the launch traced here: 34.1 us
  Pallas kernels  32.4 us (95%)
  local copies, waits for them, and re-layouts  1.67 us (5%)
    pallas_call x1, Pallas kernels, local(): pl.pallas_call(functools.partial(kernel, (n_tp, n_sp, d_conv, positions *...  32.4 us
    unnamed x1, local copies, waits for them, and re-layouts  1.67 us

profile of v1, /device:TPU:24, one launch (start us, length us, event | category | flops | bytes accessed | tf_op | source)
XLA Modules:
  0.0 34.1 jit_solution(655322117457931476)
XLA Ops:
  0.0 32.4 %shard_map.154 = bf16[1,128,1024]{2,1,0:T(8,128)(2,1)} custom-call(bf16[1,128,1024]{2,1,0:T(8,128)(2,1)} %frames.1, f32[1,1024]{1,0:T(1,128)} %bitcast.6, bf16[1024,128]{1,0:T(8,128)(2,1)} %cvw.1, bf16[1024,128]{1,0:T(8,128)(2,1)} %cgw.1, bf16[31,128]{1,0:T(8,128)(2,1)} %taps.1, f32[1,128]{1,0:T(1,128)} %bitcast.9, f32[1,128]{1,0:T(1,128)} %bitcast.10, ...), custom_call_target="tpu_custom_call" | custom-call | tf_op jit(solution)/shard_map/pallas_call | solution.py:521
  32.4 1.7 %copy.18 = bf16[1,128,1024]{2,1,0:T(8,128)(2,1)} copy(bf16[1,128,1024]{2,1,0:T(8,128)(2,1)} %shard_map.154) | data formatting | bytes 524288

commit v2 on v1

v2 whole, which is shorter than its diff:
```python
import functools

import jax
import jax.numpy as jnp
from jax import lax
from jax.experimental import pallas as pl
from jax.experimental.pallas import tpu as pltpu
from jax.sharding import PartitionSpec as P

HEAD = 128
LANES = 128
EDGE = 32
PACK = 16
SUB = 8
COLS = 256
EPS = 1e-06
MESH = pl.DeviceIdType.MESH
F32 = jnp.float32
BF16 = jnp.bfloat16


def flip(index, mask):
    out, bit = index, 1
    while bit <= mask:
        if mask & bit:
            out = out + bit - 2 * bit * ((index // bit) % 2)
        bit *= 2
    return out


def mm(a, b, dims=((1,), (0,))):
    return lax.dot_general(a, b, (dims, ((), ())), preferred_element_type=F32)


def split3(value):
    hi = value.astype(BF16)
    rest = value - hi.astype(F32)
    mid = rest.astype(BF16)
    return hi, mid, (rest - mid.astype(F32)).astype(BF16)


def kernel(
    cfg,
    frames, norm_gain, cvw, cgw, taps, conv_bias, channel_gain, channel_shift,
    qw, fw, iw, gw, rate, head_gain, cow, row,
    out,
    gath, norm_v, wfi, wc, wqg, taps_v, chan_v, head_v, ow,
    nrm, pacc, gate_in_s, cum_s, gated, edges, ext, filt, stat, stat_in, cvo, rco,
    grown_s, shrunk_s, value_s, gate_s, local_s, st, st_in, dec, dec_in, carry_out, carry_in, carried_s, acc, psend, precv,
    up, go, loc_sem, d2_send, d2_recv, fr_send, fr_recv, ed_send, ed_recv, stt_send, stt_recv, dc_send, dc_recv,
    ca_send, ca_recv, sm_send, sm_recv, pt_send, pt_recv,
):
    n_tp, n_sp, d_conv, seq_total, owners = cfg
    positions = frames.shape[1]
    conv_n, rec_n = cvw.shape[1], qw.shape[1]
    heads = rec_n // HEAD
    nx = n_tp // 2
    chunk = carry_out.shape[2]
    stride = n_sp // owners
    pieces = acc.shape[1]
    steps, slab = nrm.shape[1], nrm.shape[3]
    gate_at = max(steps - 2, 0)
    tp, sp = lax.axis_index("tp"), lax.axis_index("sp")
    core = tp % 2
    owner = sp // stride

    barrier = pltpu.get_barrier_semaphore()
    pl.semaphore_signal(barrier, inc=1, device_id={"tp": flip(tp, 1)}, device_id_type=MESH)
    for k in range(1, nx):
        pl.semaphore_signal(barrier, inc=1, device_id={"tp": flip(tp, 2 * k)}, device_id_type=MESH)
    for d in range(1, n_sp):

        @pl.when(sp + d < n_sp)
        def _():
            pl.semaphore_signal(barrier, inc=1, device_id={"sp": sp + d}, device_id_type=MESH)

    mine = pltpu.make_async_copy(frames, gath, loc_sem.at[0])
    gain_in = pltpu.make_async_copy(norm_gain, norm_v, loc_sem.at[1])

    def remote(src, dst, send, recv, **device):
        return pltpu.make_async_remote_copy(
            src_ref=src, dst_ref=dst, send_sem=send, recv_sem=recv, device_id=device, device_id_type=MESH
        )

    rec_at = 2 * conv_n
    own_rows = conv_n + rec_n
    table = {
        "fi": (wfi, ((fw, wfi.at[0, 0]), (iw, wfi.at[0, 1]))),
        "head": (head_v, ((rate, head_v.at[0, 0]), (head_gain, head_v.at[0, 1]))),
        "c": (wc, ((cvw, wc.at[0, :, pl.ds(0, conv_n)]), (cgw, wc.at[0, :, pl.ds(conv_n, conv_n)]))),
        "qg": (wqg, ((qw, wqg.at[0, 0]), (gw, wqg.at[0, 1]))),
        "taps": (taps_v, ((taps, taps_v.at[0]),)),
        "chan": (chan_v, ((conv_bias, chan_v.at[0, 0]), (channel_gain, chan_v.at[0, 1]), (channel_shift, chan_v.at[0, 2]))),
    }
    names = list(table)
    load, loaded, swap = [], {}, {}
    for n, (name, (buffer, parts)) in enumerate(table.items()):
        for ref, here in parts:
            load.append(pltpu.make_async_copy(ref, here, loc_sem.at[2 + n]))
        loaded[name] = pltpu.make_async_copy(buffer.at[1], buffer.at[0], loc_sem.at[2 + n])
        swap[name] = remote(buffer.at[0], buffer.at[1], d2_send.at[n], d2_recv.at[n], tp=flip(tp, 1))
    n = len(names)
    load.append(pltpu.make_async_copy(cow, ow.at[pl.ds(0, conv_n)], loc_sem.at[2 + n]))
    load.append(pltpu.make_async_copy(row, ow.at[pl.ds(rec_at, rec_n)], loc_sem.at[2 + n]))
    out_loaded = pltpu.make_async_copy(ow.at[pl.ds(0, own_rows)], ow.at[pl.ds(own_rows, own_rows)], loc_sem.at[2 + n])
    out_swap = [
        remote(ow.at[pl.ds(at, rows)], ow.at[pl.ds(at + rows, rows)], d2_send.at[n], d2_recv.at[n], tp=flip(tp, 1))
        for at, rows in ((0, conv_n), (rec_at, rec_n))
    ]
    out_swapped = remote(
        ow.at[pl.ds(0, own_rows)], ow.at[pl.ds(own_rows, own_rows)], d2_send.at[n], d2_recv.at[n], tp=flip(tp, 1)
    )
    mine.start()
    gain_in.start()
    for copy in load:
        copy.start()

    def normed_copy(k, c):
        return remote(
            nrm.at[0, c], nrm.at[k, c], fr_send.at[int(c > gate_at)], fr_recv.at[(k - 1) * steps + c], tp=flip(tp, 2 * k)
        )

    def sent(ref, sem):
        return remote(ref, ref, sem, sem, tp=flip(tp, 1))

    def normed_sent(late):
        count = steps - 1 - gate_at if late else gate_at + 1
        return sent(nrm.at[pl.ds(0, nx - 1), pl.ds(0, count)], fr_send.at[late])

    def send_normed():
        for k in range(1, nx):
            for c in range(steps):
                normed_copy(k, c).start()

    mine.wait()
    gain_in.wait()
    x = gath[0].astype(F32)
    mean = jnp.mean(x * x, axis=-1, keepdims=True)
    x = (x * lax.rsqrt(mean + EPS) * norm_v[...]).astype(BF16)
    for c in range(steps):
        nrm[0, c] = x[:, c * slab : (c + 1) * slab]
    pl.semaphore_wait(barrier, nx + sp)

    @pl.when(core == 0)
    def _():
        send_normed()

    for d in range(1, n_sp):

        @pl.when(sp >= d)
        def _():
            pl.semaphore_signal(up, inc=1, device_id={"sp": sp - d}, device_id_type=MESH)

    for name in names:
        loaded[name].wait()
        swap[name].start()
    out_loaded.wait()
    for copy in out_swap:
        copy.start()

    t_row = lax.broadcasted_iota(jnp.int32, (positions, positions), 0)
    t_col = lax.broadcasted_iota(jnp.int32, (positions, positions), 1)
    causal = t_col <= t_row
    lower = jnp.where(causal, 1.0, 0.0).astype(BF16)
    lower3 = jnp.concatenate([lower, lower, lower], axis=1)

    def weight(name, half, rows):
        if name == "c":
            return wc[half, rows, :]
        return wfi[half, "fi".index(name), rows, :] if name in "fi" else wqg[half, "qg".index(name), rows, :]

    places = {}
    for n, name in enumerate("fi"):
        for half in range(2):
            places[name, half] = slice((2 * n + half) * rec_n, (2 * n + half + 1) * rec_n)

    def slab_product(k, name, half, c):
        return mm(nrm[k, c], weight(name, half, slice(c * slab, (c + 1) * slab)))

    def feed(k, c):
        for (name, half), cols in places.items():
            part = slab_product(k, name, half, c)
            pacc[k - 1, :, cols] = part if c == 0 else pacc[k - 1, :, cols] + part

    def project(k, name, half):
        if k == 0 or (name, half) not in places:
            total = slab_product(k, name, half, 0)
            for c in range(1, steps):
                total = total + slab_product(k, name, half, c)
        else:
            total = pacc[k - 1, :, places[name, half]] + slab_product(k, name, half, steps - 1)
        return total.astype(BF16)

    def lanes_of(half):
        return slice(half * rec_n, (half + 1) * rec_n)

    def states(k, halves):
        raws = [project(k, "f", half) for half in halves]
        values = [project(k, "i", half) for half in halves]
        for half, forget_raw, value in zip(halves, raws, values):
            cols = lanes_of(half)
            in_gate = (head_v[half, 0] / seq_total) * jax.nn.sigmoid(-forget_raw.astype(F32))
            hi, mid, low = split3(jnp.log1p(-in_gate))
            cumulative = mm(lower3, jnp.concatenate([hi, mid, low], axis=0))
            last = cumulative[positions - 1 : positions, :]
            weighted = (in_gate * jnp.exp(last - cumulative)).astype(BF16)
            value_s[k, :, cols] = value
            last_decay = jnp.exp(last)
            for h in range(heads):
                lanes = slice(h * HEAD, (h + 1) * HEAD)
                block = mm(value[:, lanes], weighted[:, lanes], ((0,), (0,))).astype(BF16)
                for r in range(HEAD // chunk):
                    n = (half * heads + h) * (HEAD // chunk) + r
                    st[k, n] = block[r * chunk : (r + 1) * chunk]
                    dec[k, n] = last_decay[:, lanes]
            gate_in_s[k, :, cols] = in_gate
            cum_s[k, :, cols] = cumulative

    def gates(k, half):
        both = project(k, "c", half).astype(F32)
        result = (both[:, :conv_n] * jax.nn.sigmoid(both[:, conv_n:])).astype(BF16)
        cols = slice(half * conv_n, (half + 1) * conv_n)
        gated[k, :, cols] = result
        ext[k, half, EDGE : EDGE + positions] = result.astype(F32)

    def outer(k, half):
        cols = lanes_of(half)
        queries = project(k, "q", half).astype(F32)
        cumulative = cum_s[k, :, cols]
        grown_s[k, :, cols] = (queries * jnp.exp(cumulative)).astype(BF16)
        shrunk_s[k, :, cols] = (gate_in_s[k, :, cols] * jnp.exp(-cumulative)).astype(BF16)
        gate_s[k, :, cols] = project(k, "g", half)

    def within(k):
        for h in range(2 * heads):
            lanes = slice(h * HEAD, (h + 1) * HEAD)
            scores = mm(grown_s[k, :, lanes], shrunk_s[k, :, lanes], ((1,), (1,)))
            scores = jnp.where(causal, scores, 0.0).astype(BF16)
            local_s[k, :, lanes] = mm(scores, value_s[k, :, lanes])

    def slot(k, j):
        return 0 if k == 0 else 1 + (k - 1) * n_sp + j

    def state_copy(k, o):
        return remote(st.at[k, o], st_in.at[k, sp], stt_send.at[k], stt_recv.at[slot(k, sp)], sp=o * stride)

    def decay_copy(k, o):
        return remote(dec.at[k, o], dec_in.at[k, sp], dc_send.at[k], dc_recv.at[slot(k, sp)], sp=o * stride)

    def state_from(k, j):
        return remote(st.at[k, 0], st_in.at[k, j], stt_send.at[k], stt_recv.at[slot(k, j)], sp=j)

    def decay_from(k, j):
        return remote(dec.at[k, 0], dec_in.at[k, j], dc_send.at[k], dc_recv.at[slot(k, j)], sp=j)

    def wait_all(k):
        for last, count in ((False, n_sp - 2), (True, n_sp - 1)):

            @pl.when((sp == n_sp - 1) == last)
            def _():
                for ref, sem in ((st_in, stt_recv), (dec_in, dc_recv)):
                    some = ref.at[k, pl.ds(0, count)]
                    remote(some, some, sem.at[slot(k, 0)], sem.at[slot(k, 0)], sp=0).wait_recv()

    def send_states(k):
        for o in range(owners):

            @pl.when(jnp.logical_and(sp != o * stride, sp < n_sp - 1))
            def _():
                state_copy(k, o).start()
                decay_copy(k, o).start()

    def carry_copy(k, j):
        here = pl.ds(pl.multiple_of(owner * chunk, chunk), chunk)
        return remote(carry_out.at[k, j], carry_in.at[k, here], ca_send.at[k], ca_recv.at[k], sp=j)

    def owned(body):
        if stride == 1:
            body()
        else:
            pl.when(sp % stride == 0)(body)

    def scan(k, first, stop):
        def body():
            if first == 0:
                st_in[k, sp] = st[k, owner]
                dec_in[k, sp] = dec[k, owner]
                carried = jnp.zeros((chunk, HEAD), F32)
                if k == 0:
                    wait_all(k)
            else:
                carried = carried_s[k]
            for j in range(first, stop):
                carry_out[k, j] = carried.astype(BF16)
                if j > 0:

                    @pl.when(sp != j)
                    def _():
                        carry_copy(k, j).start()

                if j < n_sp - 1:
                    if k > 0:

                        @pl.when(sp != j)
                        def _():
                            state_from(k, j).wait_recv()
                            decay_from(k, j).wait_recv()

                    carried = dec_in[k, j] * carried + st_in[k, j].astype(F32)
            if stop < n_sp:
                carried_s[k] = carried
            else:
                here = pl.multiple_of(owner * chunk, chunk)
                carry_in[k, pl.ds(here, chunk), :] = carry_out[k, sp]

        owned(body)

    def wait_carry(k):
        for count, mine in ((owners - 1, True), (owners, False)):

            @pl.when(jnp.logical_and(sp > 0, (sp % stride == 0) == mine))
            def _():
                some = carry_in.at[k, pl.ds(0, count * chunk)]
                remote(some, some, ca_recv.at[k], ca_recv.at[k], sp=0).wait_recv()

    def edge_copy(k):
        return remote(gated.at[k, pl.ds(positions - EDGE, EDGE)], edges.at[k], ed_send.at[k], ed_recv.at[k], sp=sp + 1)

    def send_edge(k):
        @pl.when(sp < n_sp - 1)
        def _():
            edge_copy(k).start()

    def stat_copy(k, j):
        return remote(
            stat.at[k], stat_in.at[j, k ^ j], sm_send.at[0], sm_recv.at[(j - 1) * nx + (k ^ j)], tp=flip(tp, 2 * j)
        )

    def stat_from(k, j):
        return remote(stat.at[k], stat_in.at[j, k], sm_send.at[0], sm_recv.at[(j - 1) * nx + k], tp=flip(tp, 2 * j))

    reach = taps.shape[0] - 1

    def conv(k):
        @pl.when(sp > 0)
        def _():
            edge_copy(k).wait_recv()
            for half in range(2):
                cols = slice(half * conv_n, (half + 1) * conv_n)
                ext[k, half, 0:EDGE] = edges[k, :, cols].astype(F32)

        @pl.when(sp == 0)
        def _():
            ext[k, :, 0:EDGE] = jnp.zeros((2, EDGE, conv_n), F32)

        sums = squares = 0.0
        for half in range(2):
            cols = slice(half * conv_n, (half + 1) * conv_n)
            total = jnp.broadcast_to(chan_v[half, 0], (positions, conv_n))
            tap_rows = taps_v[half].astype(F32)
            for shift in range(SUB):
                part = None
                for start in range(EDGE - reach, EDGE + 1):
                    if start % SUB == shift:
                        low, rows = start - shift, positions + (SUB if shift else 0)
                        j = start - EDGE + reach
                        term = tap_rows[j : j + 1, :] * ext[k, half, low : low + rows]
                        part = term if part is None else part + term
                if part is not None:
                    total = total + part[shift : shift + positions]
            filt[k, :, cols] = total
            sums = sums + jnp.sum(total, axis=-1, keepdims=True)
            squares = squares + jnp.sum(total * total, axis=-1, keepdims=True)
        lane = lax.broadcasted_iota(jnp.int32, (positions, LANES), 1)
        both = jnp.where(lane == 0, sums, jnp.where(lane == 1, squares, 0.0))
        stat[k] = jnp.transpose(both)[0:8, :]
        for j in range(1, nx):
            stat_copy(k, j).start()

    def conv_norm(k):
        both = stat[k]
        for j in range(1, nx):
            stat_from(k, j).wait_recv()
            both = both + stat_in[j, k]
        both = both / d_conv
        turned = jnp.transpose(jnp.concatenate([both, jnp.zeros((LANES - 8, positions), F32)], axis=0))
        row_mean = turned[:, 0:1]
        row_var = turned[:, 1:2] - row_mean * row_mean
        scale = lax.rsqrt(row_var + EPS)
        for half in range(2):
            cols = slice(half * conv_n, (half + 1) * conv_n)
            scaled = (filt[k, :, cols] - row_mean) * scale * chan_v[half, 1] + chan_v[half, 2]
            cvo[k, :, cols] = (scaled * jax.nn.sigmoid(scaled)).astype(BF16)
        for n in range(pieces):
            acc[k, n] = mm(cvo[k], ow[0:rec_at, n * COLS : (n + 1) * COLS])

    def finish(k):
        wait_carry(k)
        for h in range(2 * heads):
            lanes = slice(h * HEAD, (h + 1) * HEAD)
            rec_raw = local_s[k, :, lanes] + mm(
                grown_s[k, :, lanes], carry_in[k, h * HEAD : (h + 1) * HEAD, :], ((1,), (1,))
            )
            mean = jnp.mean(rec_raw * rec_raw, axis=-1, keepdims=True)
            gain = head_v[h // heads, 1][:, (h % heads) * HEAD : (h % heads + 1) * HEAD]
            rec_norm = rec_raw * lax.rsqrt(mean + EPS) * gain
            gate = gate_s[k, :, lanes].astype(F32)
            rco[k, :, lanes] = (rec_norm * (gate * jax.nn.sigmoid(gate))).astype(BF16)

    def part_copy(k, n):
        return remote(
            psend.at[k, n], precv.at[k, n], pt_send.at[0], pt_recv.at[(k - 1) * pieces + n], tp=flip(tp, 2 * k)
        )

    def produce(k):
        for n in range(pieces):
            part = acc[k, n] + mm(rco[k], ow[rec_at : rec_at + 2 * rec_n, n * COLS : (n + 1) * COLS])
            if k == 0:
                acc[k, n] = part
            else:
                psend[k, n] = part.astype(BF16)
                part_copy(k, n).start()

    @pl.when(sp == 0)
    def _():
        carry_in[...] = jnp.zeros_like(carry_in)

    states(0, (0,))
    gates(0, 0)
    outer(0, 0)
    if nx > 1:

        @pl.when(core == 0)
        def _():
            normed_sent(0).wait_send()
            pl.semaphore_signal(go, inc=1, device_id={"tp": flip(tp, 1)}, device_id_type=MESH)

        @pl.when(core == 1)
        def _():
            pl.semaphore_wait(go, 1)
            send_normed()

    for name in ("fi", "head"):
        swap[name].wait_recv()
    states(0, (1,))

    @pl.when(sp < n_sp - 1)
    def _():
        pl.semaphore_wait(up, n_sp - 1 - sp)

    swap["c"].wait_recv()
    gates(0, 1)
    send_edge(0)
    send_states(0)

    def rest():
        swap["qg"].wait_recv()
        outer(0, 1)
        within(0)
        for copy in (swap["taps"], swap["chan"], out_swapped):
            copy.wait_recv()

    pl.when(core == 1)(rest)
    for k in range(1, nx):
        for c in range(steps - 1):
            normed_copy(k, c).wait_recv()
            feed(k, c)
        if k == 1:
            pl.when(core == 0)(rest)
        normed_copy(k, steps - 1).wait_recv()
        states(k, (0, 1))
        send_states(k)
        gates(k, 0)
        gates(k, 1)
        send_edge(k)
        middle = n_sp // 2
        late = sp >= middle
        pl.when(jnp.logical_not(late))(functools.partial(conv, k - 1))
        scan(k, 0, middle)
        pl.when(late)(functools.partial(conv, k - 1))
        scan(k, middle, n_sp)
        outer(k, 0)
        outer(k, 1)
        within(k)
    if nx == 1:
        pl.when(core == 0)(rest)
    conv(nx - 1)
    for k in range(1, nx):
        conv_norm(k)
    for k in range(1, nx):
        finish(k)
        produce(k)
    scan(0, 0, n_sp)
    conv_norm(0)
    finish(0)
    produce(0)

    for name in names:
        swap[name].wait_send()
    out_swapped.wait_send()
    for k in range(nx):

        @pl.when(sp < n_sp - 1)
        def _():
            edge_copy(k).wait_send()

        for count, mine in ((owners - 1, True), (owners, False)):

            @pl.when(jnp.logical_and(sp < n_sp - 1, (sp % stride == 0) == mine))
            def _():
                sent(st.at[k, pl.ds(0, count)], stt_send.at[k]).wait_send()
                sent(dec.at[k, pl.ds(0, count)], dc_send.at[k]).wait_send()

        for first, count in ((False, n_sp - 2), (True, n_sp - 1)):

            @pl.when(jnp.logical_and(sp % stride == 0, (sp == 0) == first))
            def _():
                sent(carry_out.at[k, pl.ds(0, count)], ca_send.at[k]).wait_send()

    if nx > 1:
        sent(stat_in.at[pl.ds(0, nx - 1)], sm_send.at[0]).wait_send()

        @pl.when(core == 1)
        def _():
            normed_sent(0).wait_send()

        normed_sent(1).wait_send()
        sent(psend.at[pl.ds(0, nx - 1)], pt_send.at[0]).wait_send()
    for n in range(pieces):
        total = acc[0, n]
        for k in range(1, nx):
            part_copy(k, n).wait_recv()
            total = total + precv[k, n].astype(F32)
        out[0, :, n * COLS : (n + 1) * COLS] = total.astype(BF16)


def wide(array, axis):
    extra = -array.shape[axis] % LANES
    if extra == 0:
        return array
    pads = [(0, 0)] * array.ndim
    pads[axis] = (0, extra)
    return jnp.pad(array, pads)


def local(
    n_tp, n_sp, frames, norm_gain, conv_value_w, conv_gate_w, conv_taps, conv_bias, channel_gain, channel_shift,
    query_w, forget_w, input_w, gate_w, memory_rate, head_gain, conv_out_w, rec_out_w,
):
    d_conv = conv_value_w.shape[1] * n_tp
    spt, positions, depth = frames.shape
    conv_value_w, conv_gate_w, conv_taps = (wide(a, 1) for a in (conv_value_w, conv_gate_w, conv_taps))
    conv_bias, channel_gain, channel_shift, conv_out_w = (
        wide(a, 0) for a in (conv_bias, channel_gain, channel_shift, conv_out_w)
    )
    conv_n, rec_n = conv_value_w.shape[1], query_w.shape[1]
    out_n = rec_out_w.shape[1]
    assert spt == 1 and n_tp % 2 == 0 and positions == LANES and out_n % COLS == 0 and depth % COLS == 0
    nx = n_tp // 2
    state_rows = 2 * rec_n
    owners = min(n_sp, state_rows // PACK)
    chunk = state_rows // owners
    pieces = out_n // COLS
    steps = depth // COLS
    vm = pltpu.VMEM
    sem = pltpu.SemaphoreType.DMA
    scratch = [
        vm((1, positions, depth), BF16),
        vm((1, depth), F32),
        vm((2, 2, depth, rec_n), BF16),
        vm((2, depth, 2 * conv_n), BF16),
        vm((2, 2, depth, rec_n), BF16),
        vm((2,) + conv_taps.shape, BF16),
        vm((2, 3, 1, conv_n), F32),
        vm((2, 2, 1, rec_n), F32),
        vm((2 * conv_n + 2 * rec_n, out_n), BF16),
        vm((nx, steps, positions, COLS), BF16),
        vm((max(nx - 1, 1), positions, 4 * rec_n), F32),
        vm((nx, positions, 2 * rec_n), F32),
        vm((nx, positions, 2 * rec_n), F32),
        vm((nx, positions, 2 * conv_n), BF16),
        vm((nx, EDGE, 2 * conv_n), BF16),
        vm((nx, 2, EDGE + positions, conv_n), F32),
        vm((nx, positions, 2 * conv_n), F32),
        vm((nx, 8, positions), F32),
        vm((nx, nx, 8, positions), F32),
        vm((nx, positions, 2 * conv_n), BF16),
        vm((nx, positions, 2 * rec_n), BF16),
        vm((nx, positions, 2 * rec_n), BF16),
        vm((nx, positions, 2 * rec_n), BF16),
        vm((nx, positions, 2 * rec_n), BF16),
        vm((nx, positions, 2 * rec_n), BF16),
        vm((nx, positions, 2 * rec_n), F32),
        vm((nx, owners, chunk, HEAD), BF16),
        vm((nx, n_sp, chunk, HEAD), BF16),
        vm((nx, owners, 1, HEAD), F32),
        vm((nx, n_sp, 1, HEAD), F32),
        vm((nx, n_sp, chunk, HEAD), BF16),
        vm((nx, state_rows, HEAD), BF16),
        vm((nx, chunk, HEAD), F32),
        vm((nx, pieces, positions, COLS), F32),
        vm((nx, pieces, positions, COLS), BF16),
        vm((nx, pieces, positions, COLS), BF16),
        pltpu.SemaphoreType.REGULAR,
        pltpu.SemaphoreType.REGULAR,
        sem((9,)),
        sem((7,)), sem((7,)),
        sem((2,)), sem((max(nx - 1, 1) * steps,)),
        sem((nx,)), sem((nx,)),
        sem((nx,)), sem((1 + (nx - 1) * n_sp,)),
        sem((nx,)), sem((1 + (nx - 1) * n_sp,)),
        sem((nx,)), sem((nx,)),
        sem((1,)), sem((max(nx - 1, 1) * nx,)),
        sem((1,)), sem((max(nx - 1, 1) * pieces,)),
    ]
    return pl.pallas_call(
        functools.partial(kernel, (n_tp, n_sp, d_conv, positions * n_sp, owners)),
        out_shape=pltpu.VMEM((spt, positions, out_n), BF16),
        in_specs=[pl.BlockSpec(memory_space=pltpu.HBM)] * 16,
        out_specs=pl.BlockSpec(memory_space=pltpu.VMEM),
        scratch_shapes=scratch,
        compiler_params=pltpu.CompilerParams(
            collective_id=0, has_side_effects=True, vmem_limit_bytes=56 * 1024 * 1024
        ),
    )(
        frames, norm_gain[None], conv_value_w, conv_gate_w, conv_taps, conv_bias[None], channel_gain[None],
        channel_shift[None], query_w, forget_w, input_w, gate_w, memory_rate[None], head_gain[None],
        conv_out_w, rec_out_w,
    )


def solution(mesh):
    placed = (
        P("tp", "sp", None),
        P(),
        P(None, "tp"),
        P(None, "tp"),
        P(None, "tp"),
        P("tp"),
        P("tp"),
        P("tp"),
        P(None, "tp"),
        P(None, "tp"),
        P(None, "tp"),
        P(None, "tp"),
        P("tp"),
        P("tp"),
        P("tp", None),
        P("tp", None),
    )
    return jax.shard_map(
        functools.partial(local, mesh.shape["tp"], mesh.shape["sp"]),
        mesh=mesh, in_specs=placed, out_specs=P("tp", "sp", None), check_vma=False,
    )
```

time: 34.2 us -> 27.5 us (0.80)
  Pallas kernels: 32.4 us -> 26.7 us
  local copies, waits for them, and re-layouts: 1.67 us -> 0.71 us
    pallas_call x1, Pallas kernels: 32.4 us -> 26.7 us  [local(): pl.pallas_call(functools.partial(kernel, (n_tp, n_sp, d_conv, positions *...]
    unnamed x1, local copies, waits for them, and re-layouts: 1.67 us -> 0.71 us
where the time goes in v2:
time: 27.5 us; the launch traced here: 27.4 us
  Pallas kernels  26.7 us (97%)
  local copies, waits for them, and re-layouts  0.71 us (3%)
    pallas_call x1, Pallas kernels, local(): pl.pallas_call(functools.partial(kernel, (n_tp, n_sp, d_conv, positions *...  26.7 us
    unnamed x1, local copies, waits for them, and re-layouts  0.71 us

profile of v2, /device:TPU:24, one launch (start us, length us, event | category | flops | bytes accessed | tf_op | source)
XLA Modules:
  0.0 27.4 jit_solution(13812810344878397602)
XLA Ops:
  0.0 26.7 %shard_map.154 = bf16[1,128,1024]{2,1,0:T(8,128)(2,1)S(1)} custom-call(bf16[1,128,1024]{2,1,0:T(8,128)(2,1)} %frames.1, f32[1,1024]{1,0:T(1,128)} %bitcast.6, bf16[1024,128]{1,0:T(8,128)(2,1)} %cvw.1, bf16[1024,128]{1,0:T(8,128)(2,1)} %cgw.1, bf16[31,128]{1,0:T(8,128)(2,1)} %taps.1, f32[1,128]{1,0:T(1,128)} %bitcast.9, f32[1,128]{1,0:T(1,128)} %bitcast.10, ...), custom_call_target="tpu_custom_call" | custom-call | tf_op jit(solution)/shard_map/pallas_call | solution.py:616
  26.7 0.7 %copy.18 = bf16[1,128,1024]{2,1,0:T(8,128)(2,1)} copy(bf16[1,128,1024]{2,1,0:T(8,128)(2,1)S(1)} %shard_map.154) | data formatting | bytes 524288
